TPU v7x, 512 devices: a whole 4x8x8 slice. The times are simulated.
512 devices in a mesh: sp: 64 (over z, y), fs: 4 (over x), tp: 2 (over core).
Axes of the slice: x: 4, y: 8, z: 8, core: 2. Of those that a mesh axis runs over, the one named last changes fastest.
Arguments:
- tokens: bfloat16 [4, 8192, 2048], P('fs', ('sp', 'tp')), may hold values from -6 to 6
- norm_gain: float32 [2048], replicated, may hold values from 0.1 to 1.9
- gla_query_weight: bfloat16 [2048, 512], P('sp', 'tp'), may hold values from -0.125 to 0.125
- gla_key_weight: bfloat16 [2048, 512], P('sp', 'tp'), may hold values from -0.125 to 0.125
- gla_value_weight: bfloat16 [2048, 1024], P('sp', 'tp'), may hold values from -0.125 to 0.125
- decay_down: bfloat16 [2048, 32], P('sp'), may hold values from -0.125 to 0.125
- decay_up: bfloat16 [32, 512], P(None, 'tp'), may hold values from -1 to 1
- decay_bias: float32 [512], P('tp'), may hold values from 0.5 to 12
- head_gain: float32 [128], replicated, may hold values from 0.1 to 1.9
- window_query_weight: bfloat16 [2048, 1024], P('sp', 'tp'), may hold values from -3 to 3
- window_key_weight: bfloat16 [2048, 256], P('sp', 'tp'), may hold values from -3 to 3
- window_value_weight: bfloat16 [2048, 256], P('sp', 'tp'), may hold values from -0.125 to 0.125
- sink_logit: float32 [16], P('tp'), may hold values from 3 to 7
- gla_output_weight: bfloat16 [1024, 2048], P('tp', 'sp'), may hold values from -0.125 to 0.125
- window_output_weight: bfloat16 [1024, 2048], P('tp', 'sp'), may hold values from -0.125 to 0.125
Outputs:
- mixed: bfloat16 [4, 8192, 2048], P('fs', ('sp', 'tp'))
All inputs are finite; a program needn't handle non-finite values.
Results may differ from a plain program's by a relative error of at most 0.013.
Values may be sent and summed in bfloat16 or wider, within the bound.
A program may use at most 64 MiB of HBM per device.

v0:
```python
import jax
import jax.numpy as jnp
from jax import lax
from jax.sharding import Mesh
from jax.sharding import PartitionSpec as P

KEY_DIM = 64
VALUE_DIM = 128
SWA_HEADS = 16
KV_HEADS = 4
HEAD_DIM = 64
WINDOW = 128
SPAN = 64
SP = ("sp_0", "sp_1")
SP_TP = ("sp_0", "sp_1", "tp")
EPS = 1e-06
SOFTMAX_TEMPER = 16.0
HIGH = lax.Precision.HIGHEST


def sent_to_all(value, axis):
    peers = lax.axis_size(axis)
    return lax.all_to_all(
        jnp.broadcast_to(value[None], (peers, *value.shape)), axis, 0, 0, tiled=True
    )


def laid_out(blocks, dim):
    dims = list(blocks.shape[1:])
    dims[dim] *= blocks.shape[0]
    return jnp.moveaxis(blocks, 0, dim).reshape(dims)


def gather_directly(value, axis, dim):
    blocks = sent_to_all(value, axis)
    return laid_out(blocks, dim)


def side_by_side(arrays, axis, dim, along):
    both = jnp.concatenate(arrays, axis=along)
    result, at, finished = (lax.all_gather(both, axis, axis=dim, tiled=True), 0, [])
    for a in arrays:
        finished.append(lax.slice_in_dim(result, at, at + a.shape[along], axis=along))
        at += a.shape[along]
    return tuple(finished)


def gather_turned(arrays, axis, dims):
    turned = [jnp.moveaxis(a, dim, 0) for a, dim in zip(arrays, dims)]
    both = jnp.concatenate([t.reshape(len(t), -1) for t in turned], axis=1)
    result, at, finished = (lax.all_gather(both, axis, axis=0, tiled=True), 0, [])
    for t, dim in zip(turned, dims):
        slab = result[:, at : at + t[0].size].reshape(-1, *t.shape[1:])
        finished.append(jnp.moveaxis(slab, 0, dim))
        at += t[0].size
    return tuple(finished)


def nothing_yet(value, identity):
    return jax.tree.map(
        lambda a, e: jnp.broadcast_to(jnp.asarray(e, a.dtype), a.shape), value, identity
    )


def carried_in(value, axes, combine, identity):
    before = start = nothing_yet(value, identity)
    subtotal = value
    for axis in reversed(axes):
        peers, place = (lax.axis_size(axis), lax.axis_index(axis))
        pieces = jax.tree.map(lambda part: lax.all_gather(part, axis), subtotal)
        inside, subtotal = (start, start)
        for k in range(peers):
            passed = k < place
            subtotal = combine(subtotal, jax.tree.map(lambda part: part[k], pieces))
            inside = jax.tree.map(lambda new, old: jnp.where(passed, new, old), subtotal, inside)
        before = combine(inside, before)
    return before


def passed_along(value, axis, by):
    peers = lax.axis_size(axis)
    pairs = [(i, i + by) for i in range(peers) if 0 <= i + by < peers]
    return lax.ppermute(value, axis, pairs)


def split_up(value, dim, peers):
    dims = value.shape
    blocks = value.reshape(*dims[:dim], peers, dims[dim] // peers, *dims[dim + 1 :])
    return jnp.moveaxis(blocks, dim, 0)


def summed_on_arrival(value, axis, dim):
    blocks = split_up(value, dim, lax.axis_size(axis))
    arrived = lax.all_to_all(blocks, axis, split_axis=0, concat_axis=0, tiled=True)
    return arrived.astype(jnp.float32).sum(axis=0)


def rms_rows(values, gain):
    mean_square = jnp.mean(values * values, axis=-1, keepdims=True)
    return values * lax.rsqrt(mean_square + EPS) * gain


def block_terms(query_rows, key_rows, value_rows, log_decay_rate, block_len):
    seq_len, head_count, key_width = query_rows.shape
    value_width = value_rows.shape[-1]
    block_count = seq_len // block_len
    q_scaled = query_rows.reshape(block_count, block_len, head_count, key_width) * key_width ** (
        -0.5
    )
    k_blocks = key_rows.reshape(block_count, block_len, head_count, key_width)
    v_blocks = value_rows.reshape(block_count, block_len, head_count, value_width)
    within = jnp.cumsum(
        log_decay_rate.reshape(block_count, block_len, head_count, key_width), axis=1
    )
    block_total = within[:, -1]
    q_dec = q_scaled * jnp.exp(within)
    k_dec = k_blocks * jnp.exp(-within)
    k_end = k_blocks * jnp.exp(block_total[:, None] - within)
    causal = jnp.tril(jnp.ones((block_len, block_len), dtype=bool))
    scores = jnp.einsum("nihd,njhd->nhij", q_dec, k_dec, precision=HIGH)
    scores = jnp.where(causal, scores, 0.0)
    local_out = jnp.einsum("nhij,njhe->nihe", scores, v_blocks, precision=HIGH)
    update = jnp.einsum("njhd,njhe->nhde", k_end, v_blocks, precision=HIGH)

    def advance(carried, inputs):
        update_in, decay_in = inputs
        return (decay_in[..., None] * carried + update_in, carried)

    start_state = jnp.zeros((head_count, key_width, value_width), jnp.float32)
    last_state, entering = lax.scan(advance, start_state, (update, jnp.exp(block_total)))
    return (q_dec, local_out, entering, last_state, block_total)


def window_band_mask(block_count, block_len, offset):
    query_pos = jnp.arange(block_len)[:, None] + block_len
    key_pos = jnp.arange(2 * block_len)[None, :]
    distance = query_pos - key_pos
    inside = (distance >= 0) & (distance < block_len)
    global_key = (
        offset + jnp.arange(block_count)[:, None, None] * block_len - block_len + key_pos[None]
    )
    return inside[None] & (global_key >= 0)


def window_attend(query_blocks, key_band, value_band, valid, sinks):
    scores = jnp.einsum(
        "nqhgd,nkhd->nhgqk", query_blocks, key_band, preferred_element_type=jnp.float32
    )
    scores = scores * HEAD_DIM ** (-0.5)
    scores = jnp.where(valid[:, None, None], scores, -1e30)
    sink_term = sinks[None, :, :, None, None]
    top = jnp.maximum(jnp.max(scores, axis=-1, keepdims=True), sink_term)
    expo = jnp.exp(scores - top)
    denom = jnp.sum(expo, axis=-1, keepdims=True) + jnp.exp(sink_term - top)
    weights = (expo / denom).astype(jnp.bfloat16)
    attended = jnp.einsum(
        "nhgqk,nkhd->nqhgd", weights, value_band, preferred_element_type=jnp.float32
    )
    return attended.astype(jnp.bfloat16)


def per_device(
    tokens,
    norm_gain,
    gla_query_weight,
    gla_key_weight,
    gla_value_weight,
    decay_down,
    decay_up,
    decay_bias,
    head_gain,
    window_query_weight,
    window_key_weight,
    window_value_weight,
    sink_logit,
    gla_output_weight,
    window_output_weight,
):
    seq_rows = gather_directly(tokens, "tp", 1)[0]
    tok_rows = seq_rows.shape[0]
    input_maps = side_by_side(
        (
            gla_query_weight,
            gla_key_weight,
            gla_value_weight,
            decay_down,
            window_query_weight,
            window_key_weight,
            window_value_weight,
        ),
        SP,
        0,
        1,
    )
    output_maps = gather_turned((gla_output_weight, window_output_weight), SP, (1, 1))
    normed = rms_rows(seq_rows.astype(jnp.float32), norm_gain).astype(jnp.bfloat16)

    def project(weight):
        return jnp.dot(normed, weight, preferred_element_type=jnp.float32).astype(jnp.bfloat16)

    seq_offset = lax.axis_index(SP) * tok_rows
    window_query = project(input_maps[4])
    sliding_key = project(input_maps[5])
    window_value = project(input_maps[6])
    kv_local = sliding_key.shape[1] // HEAD_DIM
    group_size = SWA_HEADS // KV_HEADS
    block_count = tok_rows // WINDOW
    edge_keys, edge_values = passed_along((sliding_key, window_value), SP, 1)

    def banded(rows, edge_rows):
        blocks = rows.reshape(block_count, WINDOW, kv_local, HEAD_DIM)
        edge_block = edge_rows.reshape(1, WINDOW, kv_local, HEAD_DIM)
        earlier = jnp.concatenate([edge_block, blocks[:-1]], axis=0)
        return jnp.concatenate([earlier, blocks], axis=1)

    query_blocks = window_query.reshape(block_count, WINDOW, kv_local, group_size, HEAD_DIM)
    valid = window_band_mask(block_count, WINDOW, seq_offset)
    sinks = sink_logit.reshape(kv_local, group_size)
    attended = window_attend(
        query_blocks,
        banded(sliding_key, edge_keys),
        banded(window_value, edge_values),
        valid,
        sinks,
    )
    window_hidden = attended.reshape(tok_rows, kv_local * group_size * HEAD_DIM)
    gla_query = project(input_maps[0])
    gla_key = project(input_maps[1])
    gla_value = project(input_maps[2])
    low_rank = project(input_maps[3])
    gate_logit_values = jnp.dot(low_rank, decay_up, preferred_element_type=jnp.float32) + decay_bias
    log_decay_rate = jax.nn.log_sigmoid(gate_logit_values) / SOFTMAX_TEMPER
    local_heads = gla_query.shape[1] // KEY_DIM
    q_dec, local_out, entering, last_state, block_total = block_terms(
        gla_query.astype(jnp.float32).reshape(tok_rows, local_heads, KEY_DIM),
        gla_key.astype(jnp.float32).reshape(tok_rows, local_heads, KEY_DIM),
        gla_value.astype(jnp.float32).reshape(tok_rows, local_heads, VALUE_DIM),
        log_decay_rate.reshape(tok_rows, local_heads, KEY_DIM),
        SPAN,
    )
    device_decay = jnp.exp(jnp.sum(block_total, axis=0))

    def combine(earlier, later):
        return (later[1][..., None] * earlier[0] + later[0], earlier[1] * later[1])

    identity = (jnp.zeros_like(last_state), jnp.ones_like(device_decay))
    incoming = carried_in((last_state, device_decay), SP, combine, identity)[0]
    before = jnp.cumsum(block_total, axis=0) - block_total
    entering_all = entering + jnp.exp(before)[..., None] * incoming[None]
    gla_out = local_out + jnp.einsum("nihd,nhde->nihe", q_dec, entering_all, precision=HIGH)
    gla_out = gla_out.reshape(tok_rows, local_heads, VALUE_DIM)
    gla_hidden = (
        rms_rows(gla_out, head_gain).astype(jnp.bfloat16).reshape(tok_rows, local_heads * VALUE_DIM)
    )
    own_rows = tok_rows // lax.axis_size("tp")
    total = jnp.dot(gla_hidden, output_maps[0], preferred_element_type=jnp.float32)
    mixed = summed_on_arrival(
        (total + jnp.dot(window_hidden, output_maps[1], preferred_element_type=jnp.float32)).astype(
            jnp.bfloat16
        ),
        "tp",
        0,
    )
    return mixed.astype(jnp.bfloat16).reshape(1, own_rows, mixed.shape[1])


def solution(mesh):
    split = Mesh(
        mesh.devices.reshape(8, 8, mesh.shape["fs"], mesh.shape["tp"]), ("sp_0", "sp_1", "fs", "tp")
    )
    return jax.shard_map(
        per_device,
        mesh=split,
        in_specs=(
            P("fs", SP_TP, None),
            P(),
            P(SP, "tp"),
            P(SP, "tp"),
            P(SP, "tp"),
            P(SP, None),
            P(None, "tp"),
            P("tp"),
            P(),
            P(SP, "tp"),
            P(SP, "tp"),
            P(SP, "tp"),
            P("tp"),
            P("tp", SP),
            P("tp", SP),
        ),
        out_specs=P("fs", SP_TP, None),
        check_vma=False,
    )
```

profile of v0, /device:TPU:1, one launch (start us, length us, event | category | flops | bytes accessed | tf_op | source)
XLA Modules:
  0.0 308.5 jit_solution(5424452987641162957)
XLA Ops:
  6.5 1.6 concatenate.12
  8.1 0.0 all-gather.8.cloned.1.call-update
  8.2 1.8 broadcast_in_dim.36
  10.0 10.3 %all-to-all-start = ((bf16[2,1,64,2048]{3,2,1,0:T(8,128)(2,1)}), bf16[2,1,64,2048]{3,2,1,0:T(8,128)(2,1)S(1)}, u32[]{:S(2)}, u32[]{:S(2)}) async-start(bf16[2,1,64,2048]{3,2,1,0:T(8,128)(2,1)} %broadcast_in_dim.36), calls=%async_computation | async-start | bytes 1048576 | tf_op jit(solution)/shard_map/all_to_all | solution.py:23
  20.3 1.4 all-to-all-done
  21.7 0.2 multiply_reduce_fusion
  21.9 0.1 rsqrt.23
  22.0 0.9 fusion.25
  22.9 89.3 %all-gather.8.cloned.1.call-done = bf16[2048,1824]{1,0:T(8,128)(2,1)} async-done(((bf16[32,1824]{1,0:T(8,128)(2,1)}), bf16[2048,1824]{1,0:T(8,128)(2,1)}) %all-gather.8.cloned.1.call-update) | async-done | bytes 7471120 | tf_op jit(solution)/shard_map/all_gather | solution.py:41
  112.2 1.6 fusion.43
  113.8 0.2 reshape_reshape.14
  114.0 0.1 fusion.82
  114.1 0.0 copy-start.4
  114.1 0.0 copy-start.5
  114.1 0.0 copy-start.7
  114.2 1.5 fusion.20
  115.7 0.2 mul.363
  115.9 1.5 fusion.18
  117.4 0.2 reshape.294
  117.6 2.0 fusion.11
  119.7 0.2 exponential_multiply_fusion
  119.9 0.4 fusion.34
  120.3 0.4 while.13
  120.3 0.1 bitcast_add_fusion.2
  120.5 0.1 bitcast_add_fusion.2
  120.6 0.0 copy-start.1
  120.7 0.6 copy-done.1
  121.3 0.0 all-gather.14.cloned.1.call-update
  121.3 0.0 all-gather.10.cloned.1.call-start
  121.4 18.4 %all-gather.2 = f32[8,4,64]{2,1,0:T(4,128)S(1)} all-gather(f32[1,4,64]{2,1,0:T(4,128)S(1)} %exponential_bitcast_fusion), channel_id=2, replica_groups=mesh['sp_0'=8,'sp_1'=8,'fs'=4,'tp'=2] {'sp_1'}, dimensions={0}, use_global_device_ids=true | all-gather | bytes 9216 | tf_op jit(solution)/shard_map/all_gather | solution.py:70
  139.8 15.8 %all-gather.14.cloned.1.call-done = f32[32,64,128]{2,1,0:T(8,128)} async-done(((f32[4,64,128]{2,1,0:T(8,128)}), f32[32,64,128]{2,1,0:T(8,128)}) %all-gather.14.cloned.1.call-update) | async-done | bytes 1048592 | tf_op jit(solution)/shard_map/all_gather | solution.py:70
  155.7 2.4 fusion.48
  158.0 0.0 all-gather.10.cloned.1.call-update
  158.1 0.0 all-gather.12.cloned.1.call-start
  158.1 0.6 pad_maximum_fusion
  158.8 0.0 all-gather.12.cloned.1.call-update
  158.8 0.1 max.30
  158.9 0.1 fusion.64
  159.1 1.9 convolution_convert_fusion.3
  160.9 2.7 collective-permute-start.1
  163.7 19.2 %all_gather.26 = f32[8,4,64]{2,1,0:T(4,128)S(1)} all-gather(f32[1,4,64]{2,1,0:T(4,128)S(1)} %get-tuple-element.80), channel_id=1, replica_groups=mesh['sp_0'=8,'sp_1'=8,'fs'=4,'tp'=2] {'sp_0'}, dimensions={0}, use_global_device_ids=true | all-gather | bytes 9216 | tf_op jit(solution)/shard_map/all_gather | solution.py:70
  182.9 0.5 convolution_select_fusion
  183.5 0.3 fusion.66
  183.7 1.9 convolution_convert_fusion.4
  185.6 2.6 fusion.14
  188.3 0.1 copy.58
  188.4 2.4 collective-permute-start
  190.8 0.4 fusion.81
  191.1 0.1 broadcast_maximum_fusion
  191.2 0.2 fusion.26
  191.4 0.1 exponential_add_fusion
  191.4 0.3 collective-permute-done
  191.8 0.3 convolution_convert_fusion
  192.1 7.2 %all-gather.10.cloned.1.call-done = f32[8,4,64,128]{3,2,1,0:T(8,128)} async-done(((f32[1,4,64,128]{3,2,1,0:T(8,128)}), f32[8,4,64,128]{3,2,1,0:T(8,128)}) %all-gather.10.cloned.1.call-update) | async-done | bytes 1048592 | tf_op jit(solution)/shard_map/all_gather | solution.py:70
  199.3 1.9 fusion.47
  201.2 0.6 multiply_reduce_fusion.1
  201.8 0.1 copy.63
  201.9 0.2 copy.55
  202.1 85.4 %all-gather.12.cloned.1.call-done = bf16[2048,1024]{1,0:T(8,128)(2,1)} async-done(((bf16[32,1024]{1,0:T(8,128)(2,1)}), bf16[2048,1024]{1,0:T(8,128)(2,1)}) %all-gather.12.cloned.1.call-update) | async-done | bytes 4194320 | tf_op jit(solution)/shard_map/all_gather | solution.py:51
  287.5 0.2 mul.428
  287.7 2.4 fusion.4
  290.1 2.4 fusion
  292.6 8.6 %all_to_all.10 = bf16[2,64,2048]{2,1,0:T(8,128)(2,1)S(1)} all-to-all(bf16[2,64,2048]{2,1,0:T(8,128)(2,1)S(1)} %bitcast.233), channel_id=1, replica_groups=mesh['sp_0'=8,'sp_1'=8,'fs'=4,'tp'=2] {'tp'}, dimensions={0} | all-to-all | bytes 1048576 | tf_op jit(solution)/shard_map/all_to_all | solution.py:94
  301.1 0.8 reduce_sum.52
  (34 shorter events, 0.2 us)
Async XLA Ops:
  6.5 105.7 %copy-start = (bf16[32,256]{1,0:T(8,128)(2,1)S(1)}, bf16[32,256]{1,0:T(8,128)(2,1)}, u32[]{:S(2)}) copy-start(bf16[32,256]{1,0:T(8,128)(2,1)} %param.23) | copy-start | bytes 49156
  6.5 105.7 %all-gather.8.cloned.1.call-start = ((), (), s32[]{:S(2)}) async-start(), calls=%async_computation.2 | async-start | bytes 7987200 | tf_op jit(solution)/shard_map/all_gather | solution.py:41
  10.0 11.7 %all-to-all-start = ((bf16[2,1,64,2048]{3,2,1,0:T(8,128)(2,1)}), bf16[2,1,64,2048]{3,2,1,0:T(8,128)(2,1)S(1)}, u32[]{:S(2)}, u32[]{:S(2)}) async-start(bf16[2,1,64,2048]{3,2,1,0:T(8,128)(2,1)} %broadcast_in_dim.36), calls=%async_computation | async-start | bytes 1048576 | tf_op jit(solution)/shard_map/all_to_all | solution.py:23
  20.3 135.4 %all-gather.14.cloned.1.call-start = ((), (), s32[]{:S(2)}) async-start(), calls=%async_computation.5 | async-start | bytes 1179648 | tf_op jit(solution)/shard_map/all_gather | solution.py:70
  114.1 44.0 %copy-start.4 = (bf16[512,32]{0,1:T(8,128)(2,1)S(1)}, bf16[512,32]{0,1:T(8,128)(2,1)}, u32[]{:S(2)}) copy-start(bf16[512,32]{0,1:T(8,128)(2,1)} %param.31) | copy-start | bytes 98308
  114.1 44.0 %copy-start.5 = (bf16[512,32]{0,1:T(8,128)(2,1)S(1)}, bf16[512,32]{0,1:T(8,128)(2,1)}, u32[]{:S(2)}) copy-start(bf16[512,32]{0,1:T(8,128)(2,1)} %param.30) | copy-start | bytes 98308
  114.1 44.7 %copy-start.7 = (f32[8]{0:T(128)S(1)}, f32[8]{0:T(128)}, u32[]{:S(2)}) copy-start(f32[8]{0:T(128)} %param.29) | copy-start | bytes 100
  114.2 44.8 %copy-start.6 = (f32[128]{0:T(128)S(1)}, f32[128]{0:T(128)}, u32[]{:S(2)}) copy-start(f32[128]{0:T(128)} %param.25) | copy-start | bytes 1540
  120.6 0.7 copy-start.1
  121.3 78.0 %all-gather.10.cloned.1.call-start = ((), (), s32[]{:S(2)}) async-start(), calls=%async_computation.3 | async-start | bytes 1179648 | tf_op jit(solution)/shard_map/all_gather | solution.py:70
  155.7 43.6 %copy-start.2 = (f32[32,64,128]{2,1,0:T(8,128)S(1)}, f32[32,64,128]{2,1,0:T(8,128)}, u32[]{:S(2)}) copy-start(f32[32,64,128]{2,1,0:T(8,128)} %all-gather.14.cloned.1.call-done) | copy-start | bytes 3145732
  158.0 41.3 %copy-start.3 = (f32[1,4,64,128]{3,2,1,0:T(8,128)S(1)}, f32[1,4,64,128]{3,2,1,0:T(8,128)}, u32[]{:S(2)}) copy-start(f32[1,4,64,128]{3,2,1,0:T(8,128)} %get-tuple-element.63) | copy-start | bytes 393220
  158.1 129.4 %all-gather.12.cloned.1.call-start = ((), (), s32[]{:S(2)}) async-start(), calls=%async_computation.4 | async-start | bytes 4259840 | tf_op jit(solution)/shard_map/all_gather | solution.py:51
  160.9 29.8 %collective-permute-start.1 = (bf16[128,128]{0,1:T(8,128)(2,1)S(1)}, bf16[128,128]{0,1:T(8,128)(2,1)S(1)}, u32[]{:S(2)}, u32[]{:S(2)}) collective-permute-start(bf16[128,128]{0,1:T(8,128)(2,1)S(1)} %convolution_convert_fusion.3), channel_id=1, source_target_pairs={{0,8},{8,16},{16,24},{24,32},{32,40},{40,48},{48,56},{56,64},{64,7... | collective-permute-start | bytes 98312 | tf_op jit(solution)/shard_map/ppermute | solution.py:83
  188.4 3.4 %collective-permute-start = (bf16[128,128]{0,1:T(8,128)(2,1)S(1)}, bf16[128,128]{0,1:T(8,128)(2,1)S(1)}, u32[]{:S(2)}, u32[]{:S(2)}) collective-permute-start(bf16[128,128]{0,1:T(8,128)(2,1)S(1)} %convolution_convert_fusion.4), channel_id=1, source_target_pairs={{0,8},{8,16},{16,24},{24,32},{32,40},{40,48},{48,56},{56,64},{64,7... | collective-permute-start | bytes 98312 | tf_op jit(solution)/shard_map/ppermute | solution.py:83
Sparse Core Ops, SparseCore 0:
  10.3 101.8 all-gather.7
  121.4 34.1 all-gather.13
  158.2 41.0 all-gather.9
  202.2 85.2 all-gather.11
where the time goes:
time: 309 us
  waiting for transfers between devices  200 us (65%)
  blocking collectives  46.2 us (15%)
  matrix products  20.4 us (7%)
  starting transfers between devices  15.5 us (5%)
  between operations  13.5 us (4%)
  other arithmetic  7.83 us (3%)
  local copies, waits for them, and re-layouts  5.43 us (2%)
    all_gather x1, waiting for transfers between devices, side_by_side(): lax.all_gather(both, axis, axis=dim, tiled=True)  89.3 us
    all_gather x1, waiting for transfers between devices, gather_turned(): lax.all_gather(both, axis, axis=0, tiled=True)  85.4 us
    all_gather x2, blocking collectives, carried_in(): pieces = jax.tree.map(lambda part: lax.all_gather(part, axis), subtotal)  37.6 us
    all_gather x2, waiting for transfers between devices, carried_in(): pieces = jax.tree.map(lambda part: lax.all_gather(part, axis), subtotal)  23.1 us
    dot_general x6, matrix products, project(): jnp.dot(normed, weight, preferred_element_type=jnp.float32)  11.5 us
    all_to_all x1, starting transfers between devices, sent_to_all(): lax.all_to_all(jnp.broadcast_to(value[None], (peers, *value.shape)), axis...  10.3 us
    all_to_all x1, blocking collectives, summed_on_arrival(): lax.all_to_all(blocks, axis, split_axis=0, concat_axis=0, tiled=True)  8.59 us
  transfers between devices with their start and end apart: 7, of which 6 were waited for; matrix products, arithmetic and copies ran while one was open for 5% of the time, Pallas kernels for 0%

commit v1 on v0

--- a/solution.py
+++ b/solution.py
@@ -48,7 +48,13 @@
 def gather_turned(arrays, axis, dims):
     turned = [jnp.moveaxis(a, dim, 0) for a, dim in zip(arrays, dims)]
     both = jnp.concatenate([t.reshape(len(t), -1) for t in turned], axis=1)
-    result, at, finished = (lax.all_gather(both, axis, axis=0, tiled=True), 0, [])
+    result, at, finished = (
+        jnp.concatenate(
+            lax.all_to_all(jnp.stack([both] * lax.axis_size(axis)), axis, 0, 0), axis=0
+        ),
+        0,
+        [],
+    )
     for t, dim in zip(turned, dims):
         slab = result[:, at : at + t[0].size].reshape(-1, *t.shape[1:])
         finished.append(jnp.moveaxis(slab, 0, dim))

time: 309 us -> 334 us (1.081)
  waiting for transfers between devices: 200 us -> 212 us
  starting transfers between devices: 15.5 us -> 26.1 us
    all_gather x1, waiting for transfers between devices: 89.3 us -> 175 us  [side_by_side(): lax.all_gather(both, axis, axis=dim, tiled=True)]
    all_gather x1 -> x0, waiting for transfers between devices: 85.4 us -> none  [gather_turned(): lax.all_gather(both, axis, axis=0, tiled=True)]
    all_gather x2, waiting for transfers between devices: 23.1 us -> 36.6 us  [carried_in(): pieces = jax.tree.map(lambda part: lax.all_gather(part, axis), subtotal)]
    all_to_all x0 -> x1, starting transfers between devices: none -> 11.2 us  [gather_turned(): lax.all_to_all(jnp.stack([both] * lax.axis_size(axis)), axis, 0, 0)]
  transfers between devices with their start and end apart: 7 -> 7, of which waited for: 6 -> 4; matrix products, arithmetic and copies ran while one was open for 5% -> 8% of each run, Pallas kernels for 0% -> 0%
where the time goes in v1:
time: 334 us; the launch traced here: 333 us
  waiting for transfers between devices  212 us (63%)
  blocking collectives  45.4 us (14%)
  starting transfers between devices  26.1 us (8%)
  matrix products  20.4 us (6%)
  between operations  13.5 us (4%)
  local copies, waits for them, and re-layouts  7.92 us (2%)
  other arithmetic  7.29 us (2%)
    all_gather x1, waiting for transfers between devices, side_by_side(): lax.all_gather(both, axis, axis=dim, tiled=True)  175 us
    all_gather x2, waiting for transfers between devices, carried_in(): pieces = jax.tree.map(lambda part: lax.all_gather(part, axis), subtotal)  36.6 us
    all_gather x2, blocking collectives, carried_in(): pieces = jax.tree.map(lambda part: lax.all_gather(part, axis), subtotal)  36.3 us
    dot_general x6, matrix products, project(): jnp.dot(normed, weight, preferred_element_type=jnp.float32)  11.5 us
    all_to_all x1, starting transfers between devices, gather_turned(): lax.all_to_all(jnp.stack([both] * lax.axis_size(axis)), axis, 0, 0)  11.2 us
    all_to_all x1, starting transfers between devices, sent_to_all(): lax.all_to_all(jnp.broadcast_to(value[None], (peers, *value.shape)), axis...  10.4 us
    all_to_all x1, blocking collectives, summed_on_arrival(): lax.all_to_all(blocks, axis, split_axis=0, concat_axis=0, tiled=True)  9.09 us
  transfers between devices with their start and end apart: 7, of which 4 were waited for; matrix products, arithmetic and copies ran while one was open for 8% of the time, Pallas kernels for 0%

profile of v1, /device:TPU:1, one launch (start us, length us, event | category | flops | bytes accessed | tf_op | source)
XLA Modules:
  0.0 333.0 jit_solution(15246262378807870528)
XLA Ops:
  6.5 1.6 concatenate.12
  8.2 0.0 all-gather.7.cloned.1.call-update
  8.2 1.9 broadcast_in_dim.36
  10.0 10.4 %all-to-all-start = ((bf16[2,1,64,2048]{3,2,1,0:T(8,128)(2,1)}), bf16[2,1,64,2048]{3,2,1,0:T(8,128)(2,1)S(1)}, u32[]{:S(2)}, u32[]{:S(2)}) async-start(bf16[2,1,64,2048]{3,2,1,0:T(8,128)(2,1)} %broadcast_in_dim.36), calls=%async_computation | async-start | bytes 1048576 | tf_op jit(solution)/shard_map/all_to_all | solution.py:23
  20.5 0.8 pad_maximum_fusion
  21.3 0.6 all-to-all-done
  21.9 2.5 stack.2
  24.3 11.2 %all-to-all-start.1 = ((bf16[64,32,1024]{2,1,0:T(8,128)(2,1)}), bf16[64,32,1024]{2,1,0:T(8,128)(2,1)}, u32[]{:S(2)}, u32[]{:S(2)}) async-start(bf16[64,32,1024]{2,1,0:T(8,128)(2,1)} %stack.2), calls=%async_computation.1 | async-start | bytes 8388608 | tf_op jit(solution)/shard_map/all_to_all | solution.py:53
  35.6 0.0 all-gather.11.cloned.1.call-start
  35.6 0.2 multiply_reduce_fusion
  35.8 0.1 rsqrt.23
  35.9 0.2 fusion.25
  36.1 0.1 fusion.64
  36.2 0.0 copy-start.6
  36.2 0.0 copy-start.7
  36.3 174.8 %all-gather.7.cloned.1.call-done = bf16[2048,1824]{1,0:T(8,128)(2,1)} async-done(((bf16[32,1824]{1,0:T(8,128)(2,1)}), bf16[2048,1824]{1,0:T(8,128)(2,1)}) %all-gather.7.cloned.1.call-update) | async-done | bytes 7471120 | tf_op jit(solution)/shard_map/all_gather | solution.py:41
  211.1 1.6 fusion.43
  212.7 0.2 reshape_reshape.14
  212.9 1.5 fusion.20
  214.4 0.2 mul.363
  214.6 1.5 fusion.18
  216.1 0.2 reshape.300
  216.3 2.0 fusion.11
  218.4 0.1 fusion.82
  218.5 0.2 exponential_multiply_fusion
  218.7 0.4 fusion.34
  219.1 0.4 while.13
  219.2 0.1 bitcast_add_fusion.2
  219.4 0.1 bitcast_add_fusion.2
  219.5 0.0 copy-start.1
  219.5 0.6 copy-done.1
  220.1 0.0 all-gather.11.cloned.1.call-update
  220.2 0.0 all-gather.9.cloned.1.call-start
  220.3 0.1 max.30
  220.4 1.9 convolution_convert_fusion.3
  222.3 3.0 collective-permute-start.1
  225.3 18.4 %all-gather.2 = f32[8,4,64]{2,1,0:T(4,128)S(1)} all-gather(f32[1,4,64]{2,1,0:T(4,128)S(1)} %exponential_bitcast_fusion), channel_id=2, replica_groups=mesh['sp_0'=8,'sp_1'=8,'fs'=4,'tp'=2] {'sp_1'}, dimensions={0}, use_global_device_ids=true | all-gather | bytes 9216 | tf_op jit(solution)/shard_map/all_gather | solution.py:76
  243.7 17.9 %all_gather.23 = f32[8,4,64]{2,1,0:T(4,128)S(1)} all-gather(f32[1,4,64]{2,1,0:T(4,128)S(1)} %get-tuple-element.80), channel_id=1, replica_groups=mesh['sp_0'=8,'sp_1'=8,'fs'=4,'tp'=2] {'sp_0'}, dimensions={0}, use_global_device_ids=true | all-gather | bytes 9216 | tf_op jit(solution)/shard_map/all_gather | solution.py:76
  261.7 0.5 convolution_select_fusion
  262.2 0.3 fusion.66
  262.5 1.9 convolution_convert_fusion.4
  264.4 0.0 all-gather.11.cloned.1.call-done
  264.4 2.4 fusion.48
  266.8 0.0 all-gather.9.cloned.1.call-update
  266.8 2.6 fusion.14
  269.5 0.1 copy.58
  269.6 1.3 collective-permute-start
  270.9 0.0 collective-permute-done.1
  270.9 0.4 fusion.81
  271.3 0.1 broadcast_maximum_fusion
  271.3 0.2 fusion.26
  271.5 0.1 exponential_add_fusion
  271.6 0.3 collective-permute-done
  271.9 0.3 convolution_convert_fusion
  272.2 36.5 %all-gather.9.cloned.1.call-done = f32[8,4,64,128]{3,2,1,0:T(8,128)} async-done(((f32[1,4,64,128]{3,2,1,0:T(8,128)}), f32[8,4,64,128]{3,2,1,0:T(8,128)}) %all-gather.9.cloned.1.call-update) | async-done | bytes 1048592 | tf_op jit(solution)/shard_map/all_gather | solution.py:76
  308.7 1.9 fusion.47
  310.6 0.6 multiply_reduce_fusion.1
  311.2 0.1 copy.63
  311.3 0.2 copy.55
  311.5 0.2 mul.428
  311.7 2.4 fusion.4
  314.1 2.4 fusion
  316.5 9.1 %all_to_all.15 = bf16[2,64,2048]{2,1,0:T(8,128)(2,1)S(1)} all-to-all(bf16[2,64,2048]{2,1,0:T(8,128)(2,1)S(1)} %bitcast.234), channel_id=1, replica_groups=mesh['sp_0'=8,'sp_1'=8,'fs'=4,'tp'=2] {'tp'}, dimensions={0} | all-to-all | bytes 1048576 | tf_op jit(solution)/shard_map/all_to_all | solution.py:100
  325.6 0.8 reduce_sum.52
  (34 shorter events, 0.2 us)
Async XLA Ops:
  6.5 204.6 %copy-start = (bf16[32,256]{1,0:T(8,128)(2,1)S(1)}, bf16[32,256]{1,0:T(8,128)(2,1)}, u32[]{:S(2)}) copy-start(bf16[32,256]{1,0:T(8,128)(2,1)} %param.23) | copy-start | bytes 49156
  6.5 29.4 %copy-start.4 = (f32[2048]{0:T(1024)S(1)}, f32[2048]{0:T(1024)}, u32[]{:S(2)}) copy-start(f32[2048]{0:T(1024)} %param.18) | copy-start | bytes 24580
  6.5 204.5 %all-gather.7.cloned.1.call-start = ((), (), s32[]{:S(2)}) async-start(), calls=%async_computation.3 | async-start | bytes 7987200 | tf_op jit(solution)/shard_map/all_gather | solution.py:41
  10.0 201.1 %copy-start.5 = (f32[256]{0:T(256)S(1)}, f32[256]{0:T(256)}, u32[]{:S(2)}) copy-start(f32[256]{0:T(256)} %param.24) | copy-start | bytes 3076
  10.0 11.8 %all-to-all-start = ((bf16[2,1,64,2048]{3,2,1,0:T(8,128)(2,1)}), bf16[2,1,64,2048]{3,2,1,0:T(8,128)(2,1)S(1)}, u32[]{:S(2)}, u32[]{:S(2)}) async-start(bf16[2,1,64,2048]{3,2,1,0:T(8,128)(2,1)} %broadcast_in_dim.36), calls=%async_computation | async-start | bytes 1048576 | tf_op jit(solution)/shard_map/all_to_all | solution.py:23
  24.3 287.2 %all-to-all-start.1 = ((bf16[64,32,1024]{2,1,0:T(8,128)(2,1)}), bf16[64,32,1024]{2,1,0:T(8,128)(2,1)}, u32[]{:S(2)}, u32[]{:S(2)}) async-start(bf16[64,32,1024]{2,1,0:T(8,128)(2,1)} %stack.2), calls=%async_computation.1 | async-start | bytes 8388608 | tf_op jit(solution)/shard_map/all_to_all | solution.py:53
  35.6 228.8 %all-gather.11.cloned.1.call-start = ((), (), s32[]{:S(2)}) async-start(), calls=%async_computation.5 | async-start | bytes 1179648 | tf_op jit(solution)/shard_map/all_gather | solution.py:76
  36.2 184.0 %copy-start.6 = (f32[128]{0:T(128)S(1)}, f32[128]{0:T(128)}, u32[]{:S(2)}) copy-start(f32[128]{0:T(128)} %param.25) | copy-start | bytes 1540
  36.2 184.0 %copy-start.7 = (f32[8]{0:T(128)S(1)}, f32[8]{0:T(128)}, u32[]{:S(2)}) copy-start(f32[8]{0:T(128)} %param.29) | copy-start | bytes 100
  219.5 0.7 copy-start.1
  220.2 88.6 %all-gather.9.cloned.1.call-start = ((), (), s32[]{:S(2)}) async-start(), calls=%async_computation.4 | async-start | bytes 1179648 | tf_op jit(solution)/shard_map/all_gather | solution.py:76
  222.3 48.6 %collective-permute-start.1 = (bf16[128,128]{0,1:T(8,128)(2,1)S(1)}, bf16[128,128]{0,1:T(8,128)(2,1)S(1)}, u32[]{:S(2)}, u32[]{:S(2)}) collective-permute-start(bf16[128,128]{0,1:T(8,128)(2,1)S(1)} %convolution_convert_fusion.3), channel_id=1, source_target_pairs={{0,8},{8,16},{16,24},{24,32},{32,40},{40,48},{48,56},{56,64},{64,7... | collective-permute-start | bytes 98312 | tf_op jit(solution)/shard_map/ppermute | solution.py:89
  264.4 44.3 %copy-start.2 = (f32[32,64,128]{2,1,0:T(8,128)S(1)}, f32[32,64,128]{2,1,0:T(8,128)}, u32[]{:S(2)}) copy-start(f32[32,64,128]{2,1,0:T(8,128)} %all-gather.11.cloned.1.call-done) | copy-start | bytes 3145732
  266.8 41.9 %copy-start.3 = (f32[1,4,64,128]{3,2,1,0:T(8,128)S(1)}, f32[1,4,64,128]{3,2,1,0:T(8,128)}, u32[]{:S(2)}) copy-start(f32[1,4,64,128]{3,2,1,0:T(8,128)} %get-tuple-element.63) | copy-start | bytes 393220
  269.6 2.3 collective-permute-start
Sparse Core Ops, SparseCore 0:
  10.3 200.6 all-gather.6
  220.3 34.1 all-gather.10
  266.9 41.7 all-gather.8
